TPU v7x, 32 devices: a whole 2x2x4 slice. The times are simulated.
32 devices in a mesh: sp: 16 (over z, y, x), tp: 2 (over core).
Axes of the slice: x: 2, y: 2, z: 4, core: 2. Of those that a mesh axis runs over, the one named last changes fastest.
Arguments:
- residual: bfloat16 [4096, 2048], P(('sp', 'tp')), may hold values from -6 to 6
- queries: bfloat16 [4096, 512], P('sp', 'tp'), may hold values from -6 to 6
- key_rows: bfloat16 [4096, 512], P('sp', 'tp'), may hold values from -6 to 6
- value_rows: bfloat16 [4096, 1024], P('sp', 'tp'), may hold values from -6 to 6
- out_gate: bfloat16 [4096, 1024], P('sp', 'tp'), may hold values from -6 to 6
- gate_logits: bfloat16 [4096, 512], P('sp', 'tp')
- head_gain: float32 [128], replicated, may hold values from 0.1 to 1.9
- out_weight: bfloat16 [1024, 2048], replicated, may hold values from -0.1875 to 0.1875
- norm_gain: float32 [2048], replicated, may hold values from 0.1 to 1.9
- routes: int32 [4096, 2], P(('sp', 'tp')), may hold values from 0 to 31, as said below
- group_score: float32 [4096], P(('sp', 'tp')), may hold values from 0.25 to 1
- expert_score: float32 [4096, 2], P(('sp', 'tp')), may hold values from 0.1 to 1
- gate_weight: bfloat16 [32, 2048, 512], P(('sp', 'tp')), may hold values from -0.125 to 0.125
- up_weight: bfloat16 [32, 2048, 512], P(('sp', 'tp')), may hold values from -0.125 to 0.125
- down_weight: bfloat16 [32, 512, 2048], P(('sp', 'tp')), may hold values from -0.25 to 0.25
Outputs:
- layer_out: bfloat16 [4096, 2048], P(('sp', 'tp'))
Inputs may be any that keep to these rules, and one draw needn't show every extreme that they name: `routes`: the two experts of a token differ and lie in one group of 8 consecutive expert numbers. In each aligned block of 128 tokens (the tokens of one device) no expert is named more than 12 times, and one expert, the same for all blocks of a draw, is named exactly 12 times in every block.
All inputs are finite; a program needn't handle non-finite values.
Results may differ from a plain program's by a relative error of at most 0.0056.
Values may be sent and summed in bfloat16 or wider, within the bound.
A program may use at most 64 MiB of HBM per device.

v0:
```python
import functools

import jax
import jax.numpy as jnp
from jax import lax
from jax.experimental import pallas as pl
from jax.experimental.pallas import tpu as pltpu
from jax.sharding import PartitionSpec as P

KEY_DIM = 64
VALUE_DIM = 128
BLOCK = 64
GROUP_SIZE = 8
MESH = pl.DeviceIdType.MESH
CHUNKS = 4


def dot(a, b):
    return jnp.dot(a, b, preferred_element_type=jnp.float32)


def silu(v):
    return v / (1.0 + jnp.exp(-v))


def layer_kernel(
    sp, tp, q_ref, k_ref, v_ref, og_ref, gl_ref, hgain_ref,
    res_ref, gain_ref, routes_ref, gscore_ref, escore_ref,
    wo_hbm, wg_hbm, wu_hbm, wd_hbm, out_ref,
    wo, wg, wu, wd, mixin, merged, normed, sbuf, rbuf, xsend, xin, ysend, yrecv, zsend, zrecv,
    msend, mrecv, gacc, uacc,
    mix_ref, qlead, within, spack, srecv, gpack, grecv, epack, ent,
    ms1, mr1, ms2, mr2, ms3, mr3, wsem, mixsem, msem_s, msem_r, s1, r1, s2, r2, s3, r3, s4, r4,
):
    rows, width = res_ref.shape
    half = v_ref.shape[1]
    experts = sp * tp
    cap = 3 * rows // experts
    quad = GROUP_SIZE // tp
    groups = sp // quad
    trow = rbuf_rows(rows, sp, tp)
    erow = groups * cap
    lanes = rbuf.shape[0]
    chunk = width // CHUNKS
    me_sp = lax.axis_index("sp")
    me_tp = lax.axis_index("tp")
    me_g = me_sp // quad
    me_q = me_sp % quad
    me_l = me_q * tp + me_tp

    weights = [
        pltpu.make_async_copy(h, v, wsem.at[i])
        for i, (h, v) in enumerate(((wo_hbm, wo), (wg_hbm, wg), (wu_hbm, wu), (wd_hbm, wd)))
    ]
    for w in weights:
        w.start()

    def far(d):
        g = lax.rem(me_g + d, groups)
        return g, (g * quad + me_q, me_tp)

    def near(d):
        l = lax.rem(me_l + d, GROUP_SIZE)
        return l, (me_g * quad + l // tp, l % tp)

    barrier = pltpu.get_barrier_semaphore()
    for d in range(1, groups):
        pl.semaphore_signal(barrier, inc=1, device_id=far(d)[1], device_id_type=MESH)
    for d in range(1, GROUP_SIZE):
        pl.semaphore_signal(barrier, inc=1, device_id=near(d)[1], device_id_type=MESH)

    def remote(src, dst, ssem, rsem, dev):
        return pltpu.make_async_remote_copy(
            src_ref=src, dst_ref=dst, send_sem=ssem, recv_sem=rsem, device_id=dev,
            device_id_type=MESH,
        )

    length, keys = q_ref.shape
    heads = keys // KEY_DIM
    blocks = length // BLOCK
    part = VALUE_DIM // quad
    logits = gl_ref[...].astype(jnp.float32)
    logs = (jnp.minimum(logits, 0.0) - jnp.log1p(jnp.exp(-jnp.abs(logits)))) / 16.0
    pos_i = lax.broadcasted_iota(jnp.int32, (length, length), 0)
    pos_j = lax.broadcasted_iota(jnp.int32, (length, length), 1)
    causal = (pos_i // BLOCK == pos_j // BLOCK) & (pos_j <= pos_i)
    running = jnp.dot(
        jnp.where(causal, 1.0, 0.0), logs,
        preferred_element_type=jnp.float32, precision=lax.Precision.HIGHEST,
    )
    split = [slice(n * BLOCK, (n + 1) * BLOCK) for n in range(blocks)]
    closing = [running[(n + 1) * BLOCK - 1 : (n + 1) * BLOCK, :] for n in range(blocks)]
    key_float = k_ref[...].astype(jnp.float32)
    key_closing = [key_float[s] * jnp.exp(closing[n] - running[s]) for n, s in enumerate(split)]
    key_end = list(key_closing)
    tail = jnp.zeros_like(closing[0])
    for n in range(blocks - 1, -1, -1):
        if n < blocks - 1:
            key_end[n] = key_closing[n] * jnp.exp(tail)
        tail = tail + closing[n]
    key_end = jnp.concatenate(key_end, axis=0).astype(jnp.bfloat16)
    low = lax.broadcasted_iota(jnp.int32, (VALUE_DIM, 2 * KEY_DIM), 1) < KEY_DIM
    for p in range(heads // 2):
        pair = slice(p * 2 * KEY_DIM, (p + 1) * 2 * KEY_DIM)
        both = [
            lax.dot_general(
                v_ref[:, h * VALUE_DIM : (h + 1) * VALUE_DIM], key_end[:, pair],
                (((0,), (0,)), ((), ())), preferred_element_type=jnp.float32,
            )
            for h in (2 * p, 2 * p + 1)
        ]
        end = jnp.where(low, both[0], both[1])
        for j in range(quad):
            spack[j, 0:part, pair] = end[j * part : (j + 1) * part]
    for j in range(quad):
        spack[j, part : part + 8, :] = jnp.broadcast_to(tail, (8, keys))
    pl.semaphore_wait(barrier, groups - 1 + GROUP_SIZE - 1)

    def side(d):
        j = lax.rem(me_q + d, quad)
        return j, (me_g * quad + j, me_tp)

    hop1 = []
    for d in range(1, quad):
        j, dev = side(d)
        hop1.append(remote(spack.at[j], srecv.at[me_q], ms1.at[d], mr1.at[d], dev))
        hop1[-1].start()
    srecv[me_q] = spack[me_q]

    query = q_ref[...].astype(jnp.float32) * KEY_DIM ** (-0.5) * jnp.exp(running)
    key_inverse = (key_float * jnp.exp(-running)).astype(jnp.bfloat16)
    query_bf = query.astype(jnp.bfloat16)
    lead = jnp.zeros_like(closing[0])
    for n, s in enumerate(split):
        qlead[s, :] = (query[s] * jnp.exp(lead)).astype(jnp.bfloat16)
        lead = lead + closing[n]
    older = []
    for n in range(1, blocks):
        pieces = []
        gap = jnp.zeros_like(closing[0])
        for m in range(n - 1, -1, -1):
            pieces.insert(0, key_closing[m] if m == n - 1 else key_closing[m] * jnp.exp(gap))
            gap = gap + closing[m]
        pieces.append(jnp.zeros((length - n * BLOCK, keys), jnp.float32))
        older.append(jnp.concatenate(pieces, axis=0).astype(jnp.bfloat16))
    lane2 = lax.broadcasted_iota(jnp.int32, (length, 2 * KEY_DIM), 1)
    nt = (((1,), (1,)), ((), ()))

    def of_head(x, h):
        keep = lane2[: x.shape[0]] < KEY_DIM if h % 2 == 0 else lane2[: x.shape[0]] >= KEY_DIM
        return jnp.where(keep, x, jnp.zeros_like(x))

    for h in range(heads):
        pair = slice(h // 2 * 2 * KEY_DIM, (h // 2 + 1) * 2 * KEY_DIM)
        mine_q = of_head(query_bf[:, pair], h)
        score = lax.dot_general(
            mine_q, key_inverse[:, pair], nt, preferred_element_type=jnp.float32
        )
        past = [jnp.zeros((BLOCK, length), jnp.float32)]
        for n in range(1, blocks):
            past.append(
                lax.dot_general(
                    mine_q[split[n]], older[n - 1][:, pair], nt,
                    preferred_element_type=jnp.float32,
                )
            )
        score = jnp.where(causal, score, jnp.concatenate(past, axis=0)).astype(jnp.bfloat16)
        hv = slice(h * VALUE_DIM, (h + 1) * VALUE_DIM)
        within[:, hv] = dot(score, v_ref[:, hv])

    for m in hop1:
        m.wait_recv()
    total = jnp.zeros((part, keys), jnp.float32)
    total_log = jnp.zeros((8, keys), jnp.float32)
    before_state, before_log = [], []
    for j in range(quad):
        before_state.append(total)
        before_log.append(total_log)
        step_log = srecv[j, part : part + 8, :]
        total = jnp.exp(step_log[0:1]) * total + srecv[j, 0:part, :]
        total_log = total_log + step_log
    gpack[0:part, :] = total
    gpack[part : part + 8, :] = total_log
    hop2 = []
    for d in range(1, groups):
        g, dev = far(d)
        hop2.append(remote(gpack, grecv.at[me_g], ms2.at[d], mr2.at[d], dev))
        hop2[-1].start()
    grecv[me_g] = gpack[...]

    sub = lax.broadcasted_iota(jnp.int32, (rows, rows), 0)
    route_t = routes_ref[...].astype(jnp.float32)
    score_t = escore_ref[...]
    scale_t = gscore_ref[...] * score_t / jnp.sum(score_t, axis=0, keepdims=True)
    columns = jnp.where(sub == 0, route_t[0:1, :], 0.0) + jnp.where(sub == 1, route_t[1:2, :], 0.0)
    columns = columns.T
    ra = columns[:, 0:1].astype(jnp.int32)
    rb = columns[:, 1:2].astype(jnp.int32)
    elane = lax.broadcasted_iota(jnp.int32, (rows, 128), 1)
    row_i = lax.broadcasted_iota(jnp.int32, (rows, rows), 0)
    col_i = lax.broadcasted_iota(jnp.int32, (rows, rows), 1)
    strict = jnp.where(col_i < row_i, 1.0, 0.0).astype(jnp.bfloat16)
    is_a = elane == ra
    is_b = elane == rb
    either = (jnp.where(is_a, 1.0, 0.0) + jnp.where(is_b, 1.0, 0.0)).astype(jnp.bfloat16)
    before = dot(strict, either)
    rank_a = jnp.sum(jnp.where(is_a, before, 0.0), axis=1, keepdims=True)
    rank_b = jnp.sum(jnp.where(is_b, before, 0.0), axis=1, keepdims=True)
    group = ra // GROUP_SIZE
    is_g = elane == group
    before_g = dot(strict, jnp.where(is_g, 1.0, 0.0).astype(jnp.bfloat16))
    rank_g = jnp.sum(jnp.where(is_g, before_g, 0.0), axis=1, keepdims=True).astype(jnp.int32)
    base = me_g * cap + 1
    code_a = ((ra % GROUP_SIZE) * erow + base).astype(jnp.float32) + rank_a
    code_b = ((rb % GROUP_SIZE) * erow + base).astype(jnp.float32) + rank_b
    values = jnp.where(elane == 0, code_a, 0.0) + jnp.where(elane == 1, code_b, 0.0)
    values_t = values.T[0:8, :]
    sub8 = lax.broadcasted_iota(jnp.int32, (8, rows), 0)
    values_t = values_t + jnp.where(sub8 == 2, scale_t[0:1, :], 0.0)
    values_t = values_t + jnp.where(sub8 == 3, scale_t[1:2, :], 0.0)
    slot_lane = lax.broadcasted_iota(jnp.int32, (rows, lanes), 1)
    mine = jnp.where(slot_lane == me_g * trow + rank_g, 1.0, 0.0)
    for g in range(groups):
        msend[g] = jnp.dot(
            values_t, jnp.where(group == g, mine, 0.0),
            preferred_element_type=jnp.float32, precision=lax.Precision.HIGHEST,
        )
    mrecv[me_g] = msend[me_g]
    metas = []
    for d in range(1, groups):
        g, dev = far(d)
        metas.append(remote(msend.at[g], mrecv.at[me_g], msem_s.at[d], msem_r.at[d], dev))
        metas[-1].start()
    gt = jnp.where(slot_lane == group * trow + rank_g, 1.0, 0.0)
    gather = gt.T.astype(jnp.bfloat16)
    gt = gt.astype(jnp.bfloat16)

    for m in hop2:
        m.wait_recv()
    state = jnp.zeros((part, keys), jnp.float32)
    for g in range(groups - 1):
        step_log = grecv[g, part : part + 1, :]
        state = jnp.where(me_g > g, jnp.exp(step_log) * state + grecv[g, 0:part, :], state)
    for j in range(quad):
        epack[j] = (jnp.exp(before_log[j][0:1]) * state + before_state[j]).astype(jnp.bfloat16)
    hop3 = []
    mine_v = pl.ds(pl.multiple_of(me_q * part, part), part)
    for d in range(1, quad):
        j, dev = side(d)
        hop3.append(remote(epack.at[j], ent.at[mine_v], ms3.at[d], mr3.at[d], dev))
        hop3[-1].start()
    ent[mine_v, :] = epack[me_q]
    for m in hop3:
        m.wait_recv()
    scans = hop1 + hop2 + hop3
    entering = ent[...]

    def finish(which):
        at = pl.ds(pl.multiple_of(which * rows, rows), rows)
        for h in range(heads):
            pair = slice(h // 2 * 2 * KEY_DIM, (h // 2 + 1) * 2 * KEY_DIM)
            hv = slice(h * VALUE_DIM, (h + 1) * VALUE_DIM)
            attended = within[at, hv] + lax.dot_general(
                of_head(qlead[at, pair], h), entering[:, pair], nt,
                preferred_element_type=jnp.float32,
            )
            mean = jnp.mean(attended * attended, axis=1, keepdims=True)
            unit = attended * lax.rsqrt(mean + 1e-06) * hgain_ref[...]
            mix_ref[at, hv] = (unit * silu(og_ref[at, hv].astype(jnp.float32))).astype(
                jnp.bfloat16
            )

    other = 1 - me_tp
    finish(other)
    mixcopy = remote(
        mix_ref.at[pl.ds(pl.multiple_of(other * rows, rows), rows)], mixin,
        mixsem.at[0], mixsem.at[1], (me_sp, other),
    )
    mixcopy.start()

    finish(me_tp)

    weights[0].wait()
    own = mix_ref[pl.ds(pl.multiple_of(me_tp * rows, rows), rows), :]
    own_w = pl.multiple_of(me_tp * half, half)
    oth_w = pl.multiple_of(other * half, half)
    cols = [pl.ds(k * chunk, chunk) for k in range(CHUNKS)]
    part = [dot(own, wo[pl.ds(own_w, half), c]) for c in cols]
    mixcopy.wait_recv()
    peer = mixin[...]
    square = jnp.zeros((rows, 1), jnp.float32)
    for k, c in enumerate(cols):
        total = part[k] + dot(peer, wo[pl.ds(oth_w, half), c])
        summed = (res_ref[:, c].astype(jnp.float32) + total).astype(jnp.bfloat16)
        merged[:, c] = summed
        wide = summed.astype(jnp.float32)
        square = square + jnp.sum(wide * wide, axis=1, keepdims=True)
    inv = lax.rsqrt(square / width + 1e-06)
    for c in cols:
        normed[:, c] = (merged[:, c].astype(jnp.float32) * inv * gain_ref[:, c]).astype(
            jnp.bfloat16
        )

    if lanes > groups * trow:
        pad = lanes - groups * trow
        rbuf[pl.ds(groups * trow, pad), :] = jnp.zeros((pad, width), jnp.bfloat16)
        zrecv[pl.ds(groups * trow, pad), :] = jnp.zeros((pad, width), jnp.bfloat16)
    far_rows = lambda g: pl.ds(pl.multiple_of(g * trow, 16), trow)
    near_rows = lambda l: pl.ds(pl.multiple_of(l * erow, 16), erow)
    sends = [mixcopy] + metas + scans

    def spread_far(k, src, dst, ss, rr):
        out = []
        for d in range(1, groups):
            g, dev = far(d)
            out.append(
                remote(
                    src.at[far_rows(g), cols[k]], dst.at[far_rows(me_g), cols[k]],
                    ss.at[k, d], rr.at[k, d], dev,
                )
            )
            out[-1].start()
        dst[far_rows(me_g), cols[k]] = src[far_rows(me_g), cols[k]]
        return out

    def spread_near(k, src, dst, ss, rr):
        out = []
        for d in range(1, GROUP_SIZE):
            l, dev = near(d)
            out.append(
                remote(
                    src.at[near_rows(l), cols[k]], dst.at[near_rows(me_l), cols[k]],
                    ss.at[k, d], rr.at[k, d], dev,
                )
            )
            out[-1].start()
        dst[near_rows(me_l), cols[k]] = src[near_rows(me_l), cols[k]]
        return out

    first = []
    for k, c in enumerate(cols):
        sbuf[:, c] = dot(gather, normed[:, c]).astype(jnp.bfloat16)
        first.append(spread_far(k, sbuf, rbuf, s1, r1))

    for m in metas:
        m.wait_recv()
    table = mrecv[0]
    for g in range(1, groups):
        table = table + mrecv[g]
    key = lax.broadcasted_iota(jnp.int32, (GROUP_SIZE * erow, lanes), 0).astype(jnp.float32) + 1.0
    hit_a = key == table[0:1, :]
    hit_b = key == table[1:2, :]
    pick = (jnp.where(hit_a, 1.0, 0.0) + jnp.where(hit_b, 1.0, 0.0)).astype(jnp.bfloat16)

    second = []
    for k, c in enumerate(cols):
        for m in first[k]:
            m.wait_recv()
        xsend[:, c] = dot(pick, rbuf[:, c]).astype(jnp.bfloat16)
        second.append(spread_near(k, xsend, xin, s2, r2))

    blend = (jnp.where(hit_a, table[2:3, :], 0.0) + jnp.where(hit_b, table[3:4, :], 0.0)).T
    blend_hi = blend.astype(jnp.bfloat16)
    blend_lo = (blend - blend_hi.astype(jnp.float32)).astype(jnp.bfloat16)
    weights[1].wait()
    weights[2].wait()
    for k, c in enumerate(cols):
        for m in second[k]:
            m.wait_recv()
        block = xin[:, c]
        if k == 0:
            gacc[...] = dot(block, wg[c, :])
            uacc[...] = dot(block, wu[c, :])
        else:
            gacc[...] += dot(block, wg[c, :])
            uacc[...] += dot(block, wu[c, :])
    inner = (silu(gacc[...]) * uacc[...]).astype(jnp.bfloat16)
    weights[3].wait()
    third = []
    for k, c in enumerate(cols):
        ysend[:, c] = dot(inner, wd[:, c]).astype(jnp.bfloat16)
        third.append(spread_near(k, ysend, yrecv, s3, r3))
    fourth = []
    for k, c in enumerate(cols):
        for m in third[k]:
            m.wait_recv()
        block = yrecv[:, c]
        zsend[:, c] = (dot(blend_hi, block) + dot(blend_lo, block)).astype(jnp.bfloat16)
        fourth.append(spread_far(k, zsend, zrecv, s4, r4))
    for k, c in enumerate(cols):
        for m in fourth[k]:
            m.wait_recv()
        out_ref[:, c] = (merged[:, c].astype(jnp.float32) + dot(gt, zrecv[:, c])).astype(
            jnp.bfloat16
        )
    for batch in first + second + third + fourth:
        sends = sends + batch
    for m in sends:
        m.wait_send()


def rbuf_rows(rows, sp, tp):
    cap = 3 * rows // (sp * tp)
    most = min(GROUP_SIZE * cap // 2, rows)
    return -(-most // 16) * 16


def layer_call(
    q, k, v, og, gl, head_gain, residual, out_weight, norm_gain, routes, group_score, expert_score, wg, wu, wd
):
    sp, tp = lax.axis_size("sp"), lax.axis_size("tp")
    rows, width = residual.shape
    groups = sp * tp // GROUP_SIZE
    cap = 3 * rows // (sp * tp)
    lanes = -(-groups * rbuf_rows(rows, sp, tp) // 128) * 128
    erows = GROUP_SIZE * groups * cap
    hidden = wg.shape[1]
    quad = GROUP_SIZE // tp
    part = VALUE_DIM // quad
    keys = q.shape[1]
    vm = pl.BlockSpec(memory_space=pltpu.VMEM)
    hb = pl.BlockSpec(memory_space=pl.ANY)
    bf = jnp.bfloat16
    dma = pltpu.SemaphoreType.DMA
    fd, nd = (CHUNKS, groups), (CHUNKS, GROUP_SIZE)
    return pl.pallas_call(
        functools.partial(layer_kernel, sp, tp),
        out_shape=jax.ShapeDtypeStruct((rows, width), bf),
        in_specs=[vm] * 11 + [hb] * 4,
        out_specs=vm,
        scratch_shapes=[
            pltpu.VMEM(out_weight.shape, bf),
            pltpu.VMEM(wg.shape, bf),
            pltpu.VMEM(wu.shape, bf),
            pltpu.VMEM(wd.shape, bf),
            pltpu.VMEM((rows, v.shape[1]), bf),
            pltpu.VMEM((rows, width), bf),
            pltpu.VMEM((rows, width), bf),
            pltpu.VMEM((lanes, width), bf),
            pltpu.VMEM((lanes, width), bf),
            pltpu.VMEM((erows, width), bf),
            pltpu.VMEM((erows, width), bf),
            pltpu.VMEM((erows, width), bf),
            pltpu.VMEM((erows, width), bf),
            pltpu.VMEM((lanes, width), bf),
            pltpu.VMEM((lanes, width), bf),
            pltpu.VMEM((groups, 8, lanes), jnp.float32),
            pltpu.VMEM((groups, 8, lanes), jnp.float32),
            pltpu.VMEM((erows, hidden), jnp.float32),
            pltpu.VMEM((erows, hidden), jnp.float32),
            pltpu.VMEM(v.shape, bf),
            pltpu.VMEM(q.shape, bf),
            pltpu.VMEM(v.shape, jnp.float32),
            pltpu.VMEM((quad, part + 8, keys), jnp.float32),
            pltpu.VMEM((quad, part + 8, keys), jnp.float32),
            pltpu.VMEM((part + 8, keys), jnp.float32),
            pltpu.VMEM((groups, part + 8, keys), jnp.float32),
            pltpu.VMEM((quad, part, keys), bf),
            pltpu.VMEM((VALUE_DIM, keys), bf),
            dma((quad,)), dma((quad,)), dma((groups,)), dma((groups,)), dma((quad,)), dma((quad,)),
            dma((4,)), dma((2,)), dma((groups,)), dma((groups,)),
            dma(fd), dma(fd), dma(nd), dma(nd), dma(nd), dma(nd), dma(fd), dma(fd),
        ],
        compiler_params=pltpu.CompilerParams(
            collective_id=0, has_side_effects=True, vmem_limit_bytes=60 * 1024 * 1024
        ),
    )(
        q, k, v, og, gl, head_gain[None, :],
        residual, norm_gain[None, :], routes.T, group_score[None, :], expert_score.T,
        out_weight, wg, wu, wd,
    )


def local(
    residual,
    queries,
    key_rows,
    value_rows,
    out_gate,
    gate_logits,
    head_gain,
    out_weight,
    norm_gain,
    routes,
    group_score,
    expert_score,
    gate_weight,
    up_weight,
    down_weight,
):
    return layer_call(
        queries, key_rows, value_rows, out_gate, gate_logits, head_gain,
        residual, out_weight, norm_gain, routes, group_score, expert_score,
        gate_weight[0], up_weight[0], down_weight[0],
    )


def solution(mesh):
    placed = (
        P(("sp", "tp"), None),
        P("sp", "tp"),
        P("sp", "tp"),
        P("sp", "tp"),
        P("sp", "tp"),
        P("sp", "tp"),
        P(),
        P(),
        P(),
        P(("sp", "tp"), None),
        P(("sp", "tp")),
        P(("sp", "tp"), None),
        P(("sp", "tp"), None, None),
        P(("sp", "tp"), None, None),
        P(("sp", "tp"), None, None),
    )
    return jax.shard_map(
        local, mesh=mesh, in_specs=placed, out_specs=P(("sp", "tp"), None), check_vma=False
    )
```

profile of v0, /device:TPU:9, one launch (start us, length us, event | category | flops | bytes accessed | tf_op | source)
XLA Modules:
  0.0 77.4 jit_solution(5183291622012079498)
XLA Ops:
  0.0 75.5 %shard_map.145 = bf16[128,2048]{1,0:T(8,128)(2,1)} custom-call(bf16[256,256]{1,0:T(8,128)(2,1)} %q_ref.1, bf16[256,256]{1,0:T(8,128)(2,1)} %k_ref.1, bf16[256,512]{1,0:T(8,128)(2,1)} %v_ref.1, bf16[256,512]{1,0:T(8,128)(2,1)} %og_ref.1, bf16[256,256]{1,0:T(8,128)(2,1)} %gl_ref.1, f32[1,128]{1,0:T(1,128)} %bitcast.14, bf16[128,2048]{1,0:T(8,128)(2,1)} %res_ref.1, ...), custom_call_target="tpu_custom_call" | custom-call | tf_op jit(solution)/shard_map/pallas_call | solution.py:426
  75.5 1.9 %copy.17 = bf16[128,2048]{1,0:T(8,128)(2,1)} copy(bf16[128,2048]{1,0:T(8,128)(2,1)} %shard_map.145) | data formatting | bytes 1048576
where the time goes:
time: 78.4 us; the launch traced here: 77.4 us
  Pallas kernels  75.5 us (96%)
  local copies, waits for them, and re-layouts  1.88 us (2%)
    pallas_call x1, Pallas kernels, layer_call(): pl.pallas_call(functools.partial(layer_kernel, sp, tp), out_shape=jax.Sha...  75.5 us
    unnamed x1, local copies, waits for them, and re-layouts  1.88 us

commit v1 on v0

--- a/solution.py
+++ b/solution.py
@@ -24,13 +24,13 @@
 
 
 def layer_kernel(
-    sp, tp, q_ref, k_ref, v_ref, og_ref, gl_ref, hgain_ref,
-    res_ref, gain_ref, routes_ref, gscore_ref, escore_ref,
-    wo_hbm, wg_hbm, wu_hbm, wd_hbm, out_ref,
-    wo, wg, wu, wd, mixin, merged, normed, sbuf, rbuf, xsend, xin, ysend, yrecv, zsend, zrecv,
+    sp, tp, gl_hbm, k_hbm, v_hbm, q_hbm, routes_hbm, gscore_hbm, escore_hbm,
+    og_hbm, hgain_hbm, res_hbm, gain_hbm, wo_hbm, wg_hbm, wu_hbm, wd_hbm, out_ref,
+    gl_ref, k_ref, v_ref, q_ref, routes_ref, gscore_ref, escore_ref,
+    og_ref, hgain_ref, res_ref, gain_ref, wo, wg, wu, wd, mixin, merged, normed, sbuf, rbuf, xsend, xin, ysend, yrecv, zsend, zrecv,
     msend, mrecv, gacc, uacc,
     mix_ref, qlead, within, spack, srecv, gpack, grecv, epack, ent,
-    ms1, mr1, ms2, mr2, ms3, mr3, wsem, mixsem, msem_s, msem_r, s1, r1, s2, r2, s3, r3, s4, r4,
+    ms1, mr1, ms2, mr2, ms3, mr3, isem, mixsem, msem_s, msem_r, s1, r1, s2, r2, s3, r3, s4, r4,
 ):
     rows, width = res_ref.shape
     half = v_ref.shape[1]
@@ -48,12 +48,14 @@
     me_q = me_sp % quad
     me_l = me_q * tp + me_tp
 
-    weights = [
-        pltpu.make_async_copy(h, v, wsem.at[i])
-        for i, (h, v) in enumerate(((wo_hbm, wo), (wg_hbm, wg), (wu_hbm, wu), (wd_hbm, wd)))
-    ]
-    for w in weights:
-        w.start()
+    pairs = (
+        (gl_hbm, gl_ref), (k_hbm, k_ref), (v_hbm, v_ref), (q_hbm, q_ref),
+        (routes_hbm, routes_ref), (gscore_hbm, gscore_ref), (escore_hbm, escore_ref),
+        (og_hbm, og_ref), (hgain_hbm, hgain_ref), (res_hbm, res_ref), (gain_hbm, gain_ref),
+        (wo_hbm, wo), (wg_hbm, wg), (wu_hbm, wu), (wd_hbm, wd),
+    )
+    loads = [pltpu.make_async_copy(h, v, isem.at[i]) for i, (h, v) in enumerate(pairs)]
+    weights = loads[11:]
 
     def far(d):
         g = lax.rem(me_g + d, groups)
@@ -68,6 +70,8 @@
         pl.semaphore_signal(barrier, inc=1, device_id=far(d)[1], device_id_type=MESH)
     for d in range(1, GROUP_SIZE):
         pl.semaphore_signal(barrier, inc=1, device_id=near(d)[1], device_id_type=MESH)
+    for w in loads:
+        w.start()
 
     def remote(src, dst, ssem, rsem, dev):
         return pltpu.make_async_remote_copy(
@@ -79,6 +83,7 @@
     heads = keys // KEY_DIM
     blocks = length // BLOCK
     part = VALUE_DIM // quad
+    loads[0].wait()
     logits = gl_ref[...].astype(jnp.float32)
     logs = (jnp.minimum(logits, 0.0) - jnp.log1p(jnp.exp(-jnp.abs(logits)))) / 16.0
     pos_i = lax.broadcasted_iota(jnp.int32, (length, length), 0)
@@ -90,6 +95,7 @@
     )
     split = [slice(n * BLOCK, (n + 1) * BLOCK) for n in range(blocks)]
     closing = [running[(n + 1) * BLOCK - 1 : (n + 1) * BLOCK, :] for n in range(blocks)]
+    loads[1].wait()
     key_float = k_ref[...].astype(jnp.float32)
     key_closing = [key_float[s] * jnp.exp(closing[n] - running[s]) for n, s in enumerate(split)]
     key_end = list(key_closing)
@@ -100,6 +106,18 @@
         tail = tail + closing[n]
     key_end = jnp.concatenate(key_end, axis=0).astype(jnp.bfloat16)
     low = lax.broadcasted_iota(jnp.int32, (VALUE_DIM, 2 * KEY_DIM), 1) < KEY_DIM
+    bf = jnp.bfloat16
+    tile = lax.broadcasted_iota(jnp.int32, (16, keys), 0)
+
+    def as_rows(factor):
+        high = factor.astype(bf).astype(jnp.float32)
+        return jnp.where(tile == 0, high, jnp.where(tile == 1, factor - high, 0.0)).astype(bf)
+
+    def factor_of(rows16):
+        wide = rows16.astype(jnp.float32)
+        return wide[0:1] + wide[1:2]
+
+    loads[2].wait()
     for p in range(heads // 2):
         pair = slice(p * 2 * KEY_DIM, (p + 1) * 2 * KEY_DIM)
         both = [
@@ -111,9 +129,10 @@
         ]
         end = jnp.where(low, both[0], both[1])
         for j in range(quad):
-            spack[j, 0:part, pair] = end[j * part : (j + 1) * part]
+            spack[j, 0:part, pair] = end[j * part : (j + 1) * part].astype(bf)
+    decay_rows = as_rows(jnp.exp(tail))
     for j in range(quad):
-        spack[j, part : part + 8, :] = jnp.broadcast_to(tail, (8, keys))
+        spack[j, part : part + 16, :] = decay_rows
     pl.semaphore_wait(barrier, groups - 1 + GROUP_SIZE - 1)
 
     def side(d):
@@ -127,6 +146,7 @@
         hop1[-1].start()
     srecv[me_q] = spack[me_q]
 
+    loads[3].wait()
     query = q_ref[...].astype(jnp.float32) * KEY_DIM ** (-0.5) * jnp.exp(running)
     key_inverse = (key_float * jnp.exp(-running)).astype(jnp.bfloat16)
     query_bf = query.astype(jnp.bfloat16)
@@ -171,16 +191,16 @@
     for m in hop1:
         m.wait_recv()
     total = jnp.zeros((part, keys), jnp.float32)
-    total_log = jnp.zeros((8, keys), jnp.float32)
-    before_state, before_log = [], []
+    total_decay = jnp.ones((1, keys), jnp.float32)
+    before_state, before_decay = [], []
     for j in range(quad):
         before_state.append(total)
-        before_log.append(total_log)
-        step_log = srecv[j, part : part + 8, :]
-        total = jnp.exp(step_log[0:1]) * total + srecv[j, 0:part, :]
-        total_log = total_log + step_log
-    gpack[0:part, :] = total
-    gpack[part : part + 8, :] = total_log
+        before_decay.append(total_decay)
+        step = factor_of(srecv[j, part : part + 16, :])
+        total = step * total + srecv[j, 0:part, :].astype(jnp.float32)
+        total_decay = total_decay * step
+    gpack[0:part, :] = total.astype(bf)
+    gpack[part : part + 16, :] = as_rows(total_decay)
     hop2 = []
     for d in range(1, groups):
         g, dev = far(d)
@@ -188,6 +208,8 @@
         hop2[-1].start()
     grecv[me_g] = gpack[...]
 
+    for w in loads[4:11]:
+        w.wait()
     sub = lax.broadcasted_iota(jnp.int32, (rows, rows), 0)
     route_t = routes_ref[...].astype(jnp.float32)
     score_t = escore_ref[...]
@@ -239,10 +261,10 @@
         m.wait_recv()
     state = jnp.zeros((part, keys), jnp.float32)
     for g in range(groups - 1):
-        step_log = grecv[g, part : part + 1, :]
-        state = jnp.where(me_g > g, jnp.exp(step_log) * state + grecv[g, 0:part, :], state)
+        step = factor_of(grecv[g, part : part + 16, :])
+        state = jnp.where(me_g > g, step * state + grecv[g, 0:part, :].astype(jnp.float32), state)
     for j in range(quad):
-        epack[j] = (jnp.exp(before_log[j][0:1]) * state + before_state[j]).astype(jnp.bfloat16)
+        epack[j] = (before_decay[j] * state + before_state[j]).astype(jnp.bfloat16)
     hop3 = []
     mine_v = pl.ds(pl.multiple_of(me_q * part, part), part)
     for d in range(1, quad):
@@ -423,12 +445,17 @@
     bf = jnp.bfloat16
     dma = pltpu.SemaphoreType.DMA
     fd, nd = (CHUNKS, groups), (CHUNKS, GROUP_SIZE)
+    inputs = (
+        gl, k, v, q, routes.T, group_score[None, :], expert_score.T,
+        og, head_gain[None, :], residual, norm_gain[None, :],
+    )
     return pl.pallas_call(
         functools.partial(layer_kernel, sp, tp),
-        out_shape=jax.ShapeDtypeStruct((rows, width), bf),
-        in_specs=[vm] * 11 + [hb] * 4,
+        out_shape=pltpu.VMEM((rows, width), bf),
+        in_specs=[hb] * 15,
         out_specs=vm,
         scratch_shapes=[
+            *[pltpu.VMEM(x.shape, x.dtype) for x in inputs],
             pltpu.VMEM(out_weight.shape, bf),
             pltpu.VMEM(wg.shape, bf),
             pltpu.VMEM(wu.shape, bf),
@@ -451,24 +478,20 @@
             pltpu.VMEM(v.shape, bf),
             pltpu.VMEM(q.shape, bf),
             pltpu.VMEM(v.shape, jnp.float32),
-            pltpu.VMEM((quad, part + 8, keys), jnp.float32),
-            pltpu.VMEM((quad, part + 8, keys), jnp.float32),
-            pltpu.VMEM((part + 8, keys), jnp.float32),
-            pltpu.VMEM((groups, part + 8, keys), jnp.float32),
+            pltpu.VMEM((quad, part + 16, keys), bf),
+            pltpu.VMEM((quad, part + 16, keys), bf),
+            pltpu.VMEM((part + 16, keys), bf),
+            pltpu.VMEM((groups, part + 16, keys), bf),
             pltpu.VMEM((quad, part, keys), bf),
             pltpu.VMEM((VALUE_DIM, keys), bf),
             dma((quad,)), dma((quad,)), dma((groups,)), dma((groups,)), dma((quad,)), dma((quad,)),
-            dma((4,)), dma((2,)), dma((groups,)), dma((groups,)),
+            dma((15,)), dma((2,)), dma((groups,)), dma((groups,)),
             dma(fd), dma(fd), dma(nd), dma(nd), dma(nd), dma(nd), dma(fd), dma(fd),
         ],
         compiler_params=pltpu.CompilerParams(
             collective_id=0, has_side_effects=True, vmem_limit_bytes=60 * 1024 * 1024
         ),
-    )(
-        q, k, v, og, gl, head_gain[None, :],
-        residual, norm_gain[None, :], routes.T, group_score[None, :], expert_score.T,
-        out_weight, wg, wu, wd,
-    )
+    )(*inputs, out_weight, wg, wu, wd)
 
 
 def local(

time: 78.4 us -> 74.3 us (0.948)
  Pallas kernels: 75.5 us -> 72.1 us
  local copies, waits for them, and re-layouts: 1.88 us -> 0.8 us
    pallas_call x1, Pallas kernels: 75.5 us -> 72.1 us  [layer_call(): pl.pallas_call(functools.partial(layer_kernel, sp, tp), out_shape=pltpu.V...]
    unnamed x1, local copies, waits for them, and re-layouts: 1.88 us -> 0.8 us
where the time goes in v1:
time: 74.3 us; the launch traced here: 72.9 us
  Pallas kernels  72.1 us (97%)
  local copies, waits for them, and re-layouts  0.8 us (1%)
    pallas_call x1, Pallas kernels, layer_call(): pl.pallas_call(functools.partial(layer_kernel, sp, tp), out_shape=pltpu.V...  72.1 us

profile of v1, /device:TPU:9, one launch (start us, length us, event | category | flops | bytes accessed | tf_op | source)
XLA Modules:
  0.0 72.9 jit_solution(17567680879613312999)
XLA Ops:
  0.0 72.1 %shard_map.145 = bf16[128,2048]{1,0:T(8,128)(2,1)S(1)} custom-call(bf16[256,256]{1,0:T(8,128)(2,1)} %gl_hbm.1, bf16[256,256]{1,0:T(8,128)(2,1)} %k_hbm.1, bf16[256,512]{1,0:T(8,128)(2,1)} %v_hbm.1, bf16[256,256]{1,0:T(8,128)(2,1)} %q_hbm.1, s32[2,128]{1,0:T(2,128)} %bitcast.12, f32[1,128]{1,0:T(1,128)} %bitcast.14, f32[2,128]{1,0:T(2,128)} %bitcast.13, ...), custom_call_target="tpu_custom_call" | custom-call | tf_op jit(solution)/shard_map/pallas_call | solution.py:452
  72.1 0.8 %copy.17 = bf16[128,2048]{1,0:T(8,128)(2,1)} copy(bf16[128,2048]{1,0:T(8,128)(2,1)S(1)} %shard_map.145) | data formatting | bytes 1048576

commit v2 on v1

--- a/solution.py
+++ b/solution.py
@@ -13,6 +13,8 @@
 GROUP_SIZE = 8
 MESH = pl.DeviceIdType.MESH
 CHUNKS = 4
+UNITS = 4
+TILE = 16
 
 
 def dot(a, b):
@@ -28,7 +30,7 @@
     og_hbm, hgain_hbm, res_hbm, gain_hbm, wo_hbm, wg_hbm, wu_hbm, wd_hbm, out_ref,
     gl_ref, k_ref, v_ref, q_ref, routes_ref, gscore_ref, escore_ref,
     og_ref, hgain_ref, res_ref, gain_ref, wo, wg, wu, wd, mixin, merged, normed, sbuf, rbuf, xsend, xin, ysend, yrecv, zsend, zrecv,
-    msend, mrecv, gacc, uacc,
+    msend, mrecv,
     mix_ref, qlead, within, spack, srecv, gpack, grecv, epack, ent,
     ms1, mr1, ms2, mr2, ms3, mr3, isem, mixsem, msem_s, msem_r, s1, r1, s2, r2, s3, r3, s4, r4,
 ):
@@ -39,8 +41,12 @@
     quad = GROUP_SIZE // tp
     groups = sp // quad
     trow = rbuf_rows(rows, sp, tp)
-    erow = groups * cap
-    lanes = rbuf.shape[0]
+    per = groups // UNITS
+    slots = per * cap
+    bulk = width * slots // TILE
+    narrow = width - bulk
+    packs = bulk // narrow
+    lanes = sbuf.shape[0]
     chunk = width // CHUNKS
     me_sp = lax.axis_index("sp")
     me_tp = lax.axis_index("tp")
@@ -232,16 +238,15 @@
     is_g = elane == group
     before_g = dot(strict, jnp.where(is_g, 1.0, 0.0).astype(jnp.bfloat16))
     rank_g = jnp.sum(jnp.where(is_g, before_g, 0.0), axis=1, keepdims=True).astype(jnp.int32)
-    base = me_g * cap + 1
-    code_a = ((ra % GROUP_SIZE) * erow + base).astype(jnp.float32) + rank_a
-    code_b = ((rb % GROUP_SIZE) * erow + base).astype(jnp.float32) + rank_b
+    code_a = ((ra % GROUP_SIZE) * cap + 1).astype(jnp.float32) + rank_a
+    code_b = ((rb % GROUP_SIZE) * cap + 1).astype(jnp.float32) + rank_b
     values = jnp.where(elane == 0, code_a, 0.0) + jnp.where(elane == 1, code_b, 0.0)
     values_t = values.T[0:8, :]
     sub8 = lax.broadcasted_iota(jnp.int32, (8, rows), 0)
     values_t = values_t + jnp.where(sub8 == 2, scale_t[0:1, :], 0.0)
     values_t = values_t + jnp.where(sub8 == 3, scale_t[1:2, :], 0.0)
     slot_lane = lax.broadcasted_iota(jnp.int32, (rows, lanes), 1)
-    mine = jnp.where(slot_lane == me_g * trow + rank_g, 1.0, 0.0)
+    mine = jnp.where(elane == rank_g, 1.0, 0.0)
     for g in range(groups):
         msend[g] = jnp.dot(
             values_t, jnp.where(group == g, mine, 0.0),
@@ -325,100 +330,193 @@
 
     if lanes > groups * trow:
         pad = lanes - groups * trow
-        rbuf[pl.ds(groups * trow, pad), :] = jnp.zeros((pad, width), jnp.bfloat16)
-        zrecv[pl.ds(groups * trow, pad), :] = jnp.zeros((pad, width), jnp.bfloat16)
+        zrecv[pl.ds(groups * trow, pad), :] = jnp.zeros((pad, width), bf)
     far_rows = lambda g: pl.ds(pl.multiple_of(g * trow, 16), trow)
-    near_rows = lambda l: pl.ds(pl.multiple_of(l * erow, 16), erow)
+    near_rows = lambda l: pl.ds(pl.multiple_of(l * TILE, TILE), TILE)
     sends = [mixcopy] + metas + scans
-
-    def spread_far(k, src, dst, ss, rr):
-        out = []
-        for d in range(1, groups):
-            g, dev = far(d)
-            out.append(
-                remote(
-                    src.at[far_rows(g), cols[k]], dst.at[far_rows(me_g), cols[k]],
-                    ss.at[k, d], rr.at[k, d], dev,
-                )
+    order = arrival_order(me_g, groups)
+
+    def home(g):
+        return (g * quad + me_q, me_tp)
+
+    def from_far(i):
+        return remote(
+            sbuf.at[far_rows(order[i])], rbuf.at[far_rows(order[i])],
+            s1.at[i], r1.at[order[i]], home(order[i]),
+        )
+
+    sbuf[...] = dot(gather, normed[...]).astype(bf)
+    for i, g in enumerate(send_order(me_g, groups)):
+        sends.append(
+            remote(
+                sbuf.at[far_rows(g)], rbuf.at[far_rows(me_g)], s1.at[i], r1.at[me_g], home(g)
             )
-            out[-1].start()
-        dst[far_rows(me_g), cols[k]] = src[far_rows(me_g), cols[k]]
-        return out
-
-    def spread_near(k, src, dst, ss, rr):
+        )
+        sends[-1].start()
+    rbuf[far_rows(me_g), :] = sbuf[far_rows(me_g), :]
+    for m in metas:
+        m.wait_recv()
+
+    slab = GROUP_SIZE * TILE
+    parts = [pl.ds(t * narrow, narrow) for t in range(packs)]
+    last = pl.ds(bulk, narrow)
+
+    def keys_of(row, t, p):
+        at = row % TILE
+        slot = at if t is None else packs * (at - slots) + t
+        valid = at < slots if t is None else at >= slots
+        if per > 1:
+            valid = valid & (slot // cap == p)
+        return jnp.where(valid, (row // TILE) * cap + slot - p * cap + 1, -1).astype(jnp.float32)
+
+    down_row = lax.broadcasted_iota(jnp.int32, (slab, trow), 0)
+    across_row = lax.broadcasted_iota(jnp.int32, (trow, slab), 1)
+    sq_i = lax.broadcasted_iota(jnp.int32, (slab, slab), 0)
+    sq_j = lax.broadcasted_iota(jnp.int32, (slab, slab), 1)
+
+    def pairs_of(packed, plain, t):
+        same = packed // TILE == plain // TILE
+        at = packed % TILE
+        hit = same & (at >= slots) & (plain % TILE == packs * (at - slots) + t)
+        return jnp.where(hit & (plain % TILE < slots), 1.0, 0.0).astype(bf)
+
+    unpack = [pairs_of(sq_j, sq_i, t) for t in range(packs)]
+    repack = [pairs_of(sq_i, sq_j, t) for t in range(packs)]
+    plain_row = lax.broadcasted_iota(jnp.int32, (slab, narrow), 0) % TILE < slots
+
+    def spread(u, src, dst, ss, rr):
         out = []
         for d in range(1, GROUP_SIZE):
             l, dev = near(d)
             out.append(
                 remote(
-                    src.at[near_rows(l), cols[k]], dst.at[near_rows(me_l), cols[k]],
-                    ss.at[k, d], rr.at[k, d], dev,
+                    src.at[u, near_rows(l)], dst.at[u, near_rows(me_l)],
+                    ss.at[u, d], rr.at[u, d], dev,
                 )
             )
             out[-1].start()
-        dst[near_rows(me_l), cols[k]] = src[near_rows(me_l), cols[k]]
+        dst[u, near_rows(me_l), :] = src[u, near_rows(me_l), :]
+        sends.extend(out)
         return out
 
-    first = []
-    for k, c in enumerate(cols):
-        sbuf[:, c] = dot(gather, normed[:, c]).astype(jnp.bfloat16)
-        first.append(spread_far(k, sbuf, rbuf, s1, r1))
-
-    for m in metas:
-        m.wait_recv()
-    table = mrecv[0]
-    for g in range(1, groups):
-        table = table + mrecv[g]
-    key = lax.broadcasted_iota(jnp.int32, (GROUP_SIZE * erow, lanes), 0).astype(jnp.float32) + 1.0
-    hit_a = key == table[0:1, :]
-    hit_b = key == table[1:2, :]
-    pick = (jnp.where(hit_a, 1.0, 0.0) + jnp.where(hit_b, 1.0, 0.0)).astype(jnp.bfloat16)
-
-    second = []
-    for k, c in enumerate(cols):
-        for m in first[k]:
+    def dispatch(u):
+        acc = [jnp.zeros((slab, narrow), jnp.float32) for _ in range(packs)]
+        for p in range(per):
+            i = u * per + p
+            if i > 0:
+                from_far(i).wait_recv()
+            table = mrecv[order[i]][:, 0:trow]
+
+            def pick(t):
+                key = keys_of(down_row, t, p)
+                hit = (key == table[0:1, :]) | (key == table[1:2, :])
+                return jnp.where(hit, 1.0, 0.0).astype(bf)
+
+            plain = pick(None)
+            tail_cols = rbuf[far_rows(order[i]), last]
+            for t in range(packs):
+                acc[t] = acc[t] + dot(plain, rbuf[far_rows(order[i]), parts[t]])
+                acc[t] = acc[t] + dot(pick(t), tail_cols)
+        for t in range(packs):
+            xsend[u, :, parts[t]] = acc[t].astype(bf)
+        return spread(u, xsend, xin, s2, r2)
+
+    def experts(u, arriving):
+        for m in arriving:
             m.wait_recv()
-        xsend[:, c] = dot(pick, rbuf[:, c]).astype(jnp.bfloat16)
-        second.append(spread_near(k, xsend, xin, s2, r2))
-
-    blend = (jnp.where(hit_a, table[2:3, :], 0.0) + jnp.where(hit_b, table[3:4, :], 0.0)).T
-    blend_hi = blend.astype(jnp.bfloat16)
-    blend_lo = (blend - blend_hi.astype(jnp.float32)).astype(jnp.bfloat16)
+        block = xin[u]
+        rest = jnp.zeros((slab, narrow), jnp.float32)
+        for t in range(packs):
+            rest = rest + dot(unpack[t], xin[u, :, parts[t]])
+        rest = rest.astype(bf)
+        gated = dot(block, wg[0:bulk, :]) + dot(rest, wg[bulk:width, :])
+        lifted = dot(block, wu[0:bulk, :]) + dot(rest, wu[bulk:width, :])
+        inner = (silu(gated) * lifted).astype(bf)
+        ends = dot(inner, wd[:, last]).astype(bf)
+        for t in range(packs):
+            main = dot(inner, wd[:, parts[t]])
+            ysend[u, :, parts[t]] = jnp.where(plain_row, main, dot(repack[t], ends)).astype(bf)
+
+    def give_back(u):
+        return spread(u, ysend, yrecv, s3, r3)
+
+    def combine(u, arriving):
+        for m in arriving:
+            m.wait_recv()
+        for p in range(per):
+            i = u * per + p
+            table = mrecv[order[i]].T[0:trow, :]
+
+            def blend(t):
+                key = keys_of(across_row, t, p)
+                both = jnp.where(key == table[:, 0:1], table[:, 2:3], 0.0)
+                both = both + jnp.where(key == table[:, 1:2], table[:, 3:4], 0.0)
+                high = both.astype(bf)
+                return [high, (both - high.astype(jnp.float32)).astype(bf)]
+
+            plain = blend(None)
+            ends = jnp.zeros((trow, narrow), jnp.float32)
+            to = zrecv if i == 0 else zsend
+            for t in range(packs):
+                four = dot(jnp.concatenate(plain + blend(t), axis=0), yrecv[u, :, parts[t]])
+                to[far_rows(order[i]), parts[t]] = (four[0:trow] + four[trow : 2 * trow]).astype(bf)
+                ends = ends + four[2 * trow : 3 * trow] + four[3 * trow : 4 * trow]
+            to[far_rows(order[i]), last] = ends.astype(bf)
+            if i > 0:
+                sends.append(
+                    remote(
+                        zsend.at[far_rows(order[i])], zrecv.at[far_rows(me_g)],
+                        s4.at[i], r4.at[me_g], home(order[i]),
+                    )
+                )
+                sends[-1].start()
+
+    out0 = dispatch(0)
     weights[1].wait()
     weights[2].wait()
-    for k, c in enumerate(cols):
-        for m in second[k]:
-            m.wait_recv()
-        block = xin[:, c]
-        if k == 0:
-            gacc[...] = dot(block, wg[c, :])
-            uacc[...] = dot(block, wu[c, :])
-        else:
-            gacc[...] += dot(block, wg[c, :])
-            uacc[...] += dot(block, wu[c, :])
-    inner = (silu(gacc[...]) * uacc[...]).astype(jnp.bfloat16)
     weights[3].wait()
-    third = []
-    for k, c in enumerate(cols):
-        ysend[:, c] = dot(inner, wd[:, c]).astype(jnp.bfloat16)
-        third.append(spread_near(k, ysend, yrecv, s3, r3))
-    fourth = []
-    for k, c in enumerate(cols):
-        for m in third[k]:
-            m.wait_recv()
-        block = yrecv[:, c]
-        zsend[:, c] = (dot(blend_hi, block) + dot(blend_lo, block)).astype(jnp.bfloat16)
-        fourth.append(spread_far(k, zsend, zrecv, s4, r4))
-    for k, c in enumerate(cols):
-        for m in fourth[k]:
-            m.wait_recv()
-        out_ref[:, c] = (merged[:, c].astype(jnp.float32) + dot(gt, zrecv[:, c])).astype(
-            jnp.bfloat16
-        )
-    for batch in first + second + third + fourth:
-        sends = sends + batch
+    experts(0, out0)
+    out1 = dispatch(1)
+    out2 = dispatch(2)
+    experts(1, out1)
+    out3 = dispatch(3)
+    back1 = give_back(1)
+    experts(2, out2)
+    back2 = give_back(2)
+    experts(3, out3)
+    back3 = give_back(3)
+    back0 = give_back(0)
+    combine(1, back1)
+    combine(2, back2)
+    combine(3, back3)
+    combine(0, back0)
+    for i in range(1, groups):
+        g = order[i]
+        remote(
+            zsend.at[far_rows(g)], zrecv.at[far_rows(g)], s4.at[i], r4.at[g], home(g)
+        ).wait_recv()
+    for c in cols:
+        out_ref[:, c] = (merged[:, c].astype(jnp.float32) + dot(gt, zrecv[:, c])).astype(bf)
     for m in sends:
         m.wait_send()
+
+
+def by_place(me, rows):
+    odd, high = me % 2, me // 2
+    ones = [(1 - odd) * (1 - high), odd * (1 - high), (1 - odd) * high, odd * high]
+    return [sum(one * row[i] for one, row in zip(ones, rows)) for i in range(len(rows[0]))]
+
+
+def send_order(me, count):
+    if count != 4:
+        return [lax.rem(me + d, count) for d in range(1, count)]
+    return by_place(me, ((3, 1, 2), (3, 2, 0), (0, 1, 3), (0, 2, 1)))
+
+
+def arrival_order(me, count):
+    if count != 4:
+        return [me] + [lax.rem(me + count - d, count) for d in range(1, count)]
+    return [me] + by_place(me, ((3, 2, 1), (0, 3, 2), (3, 0, 1), (0, 1, 2)))
 
 
 def rbuf_rows(rows, sp, tp):
@@ -435,8 +533,7 @@
     groups = sp * tp // GROUP_SIZE
     cap = 3 * rows // (sp * tp)
     lanes = -(-groups * rbuf_rows(rows, sp, tp) // 128) * 128
-    erows = GROUP_SIZE * groups * cap
-    hidden = wg.shape[1]
+    slab = (UNITS, GROUP_SIZE * TILE, width * (groups // UNITS) * cap // TILE)
     quad = GROUP_SIZE // tp
     part = VALUE_DIM // quad
     keys = q.shape[1]
@@ -444,7 +541,7 @@
     hb = pl.BlockSpec(memory_space=pl.ANY)
     bf = jnp.bfloat16
     dma = pltpu.SemaphoreType.DMA
-    fd, nd = (CHUNKS, groups), (CHUNKS, GROUP_SIZE)
+    fd, nd = (groups,), (UNITS, GROUP_SIZE)
     inputs = (
         gl, k, v, q, routes.T, group_score[None, :], expert_score.T,
         og, head_gain[None, :], residual, norm_gain[None, :],
@@ -465,16 +562,14 @@
             pltpu.VMEM((rows, width), bf),
             pltpu.VMEM((lanes, width), bf),
             pltpu.VMEM((lanes, width), bf),
-            pltpu.VMEM((erows, width), bf),
-            pltpu.VMEM((erows, width), bf),
-            pltpu.VMEM((erows, width), bf),
-            pltpu.VMEM((erows, width), bf),
+            pltpu.VMEM(slab, bf),
+            pltpu.VMEM(slab, bf),
+            pltpu.VMEM(slab, bf),
+            pltpu.VMEM(slab, bf),
             pltpu.VMEM((lanes, width), bf),
             pltpu.VMEM((lanes, width), bf),
-            pltpu.VMEM((groups, 8, lanes), jnp.float32),
-            pltpu.VMEM((groups, 8, lanes), jnp.float32),
-            pltpu.VMEM((erows, hidden), jnp.float32),
-            pltpu.VMEM((erows, hidden), jnp.float32),
+            pltpu.VMEM((groups, 8, 128), jnp.float32),
+            pltpu.VMEM((groups, 8, 128), jnp.float32),
             pltpu.VMEM(v.shape, bf),
             pltpu.VMEM(q.shape, bf),
             pltpu.VMEM(v.shape, jnp.float32),

time: 74.3 us -> 67.7 us (0.911); the launches traced: 72.9 us -> 67.5 us
  Pallas kernels: 72.1 us -> 66.7 us
    pallas_call x1, Pallas kernels: 72.1 us -> 66.7 us  [layer_call(): pl.pallas_call(functools.partial(layer_kernel, sp, tp), out_shape=pltpu.V...]
where the time goes in v2:
time: 67.7 us; the launch traced here: 67.5 us
  Pallas kernels  66.7 us (99%)
  local copies, waits for them, and re-layouts  0.8 us (1%)
    pallas_call x1, Pallas kernels, layer_call(): pl.pallas_call(functools.partial(layer_kernel, sp, tp), out_shape=pltpu.V...  66.7 us

profile of v2, /device:TPU:9, one launch (start us, length us, event | category | flops | bytes accessed | tf_op | source)
XLA Modules:
  0.0 67.5 jit_solution(12671198615703352796)
XLA Ops:
  0.0 66.7 %shard_map.145 = bf16[128,2048]{1,0:T(8,128)(2,1)S(1)} custom-call(bf16[256,256]{1,0:T(8,128)(2,1)} %gl_hbm.1, bf16[256,256]{1,0:T(8,128)(2,1)} %k_hbm.1, bf16[256,512]{1,0:T(8,128)(2,1)} %v_hbm.1, bf16[256,256]{1,0:T(8,128)(2,1)} %q_hbm.1, s32[2,128]{1,0:T(2,128)} %bitcast.12, f32[1,128]{1,0:T(1,128)} %bitcast.14, f32[2,128]{1,0:T(2,128)} %bitcast.13, ...), custom_call_target="tpu_custom_call" | custom-call | tf_op jit(solution)/shard_map/pallas_call | solution.py:549
  66.7 0.8 %copy.17 = bf16[128,2048]{1,0:T(8,128)(2,1)} copy(bf16[128,2048]{1,0:T(8,128)(2,1)S(1)} %shard_map.145) | data formatting | bytes 1048576

commit v3 on v2

--- a/solution.py
+++ b/solution.py
@@ -145,11 +145,16 @@
         j = lax.rem(me_q + d, quad)
         return j, (me_g * quad + j, me_tp)
 
-    hop1 = []
+    beside = side(1)[1]
+
+    def batch(src, dst, ss, rr):
+        return remote(src, dst, ss, rr, beside)
+
     for d in range(1, quad):
         j, dev = side(d)
-        hop1.append(remote(spack.at[j], srecv.at[me_q], ms1.at[d], mr1.at[d], dev))
-        hop1[-1].start()
+        remote(spack.at[j], srecv.at[me_q], ms1.at[0], mr1.at[0], dev).start()
+    others = pl.ds(0, quad - 1)
+    hop1 = batch(spack.at[others], srecv.at[others], ms1.at[0], mr1.at[0])
     srecv[me_q] = spack[me_q]
 
     loads[3].wait()
@@ -194,8 +199,7 @@
         hv = slice(h * VALUE_DIM, (h + 1) * VALUE_DIM)
         within[:, hv] = dot(score, v_ref[:, hv])
 
-    for m in hop1:
-        m.wait_recv()
+    hop1.wait_recv()
     total = jnp.zeros((part, keys), jnp.float32)
     total_decay = jnp.ones((1, keys), jnp.float32)
     before_state, before_decay = [], []
@@ -207,11 +211,11 @@
         total_decay = total_decay * step
     gpack[0:part, :] = total.astype(bf)
     gpack[part : part + 16, :] = as_rows(total_decay)
-    hop2 = []
     for d in range(1, groups):
         g, dev = far(d)
-        hop2.append(remote(gpack, grecv.at[me_g], ms2.at[d], mr2.at[d], dev))
-        hop2[-1].start()
+        remote(gpack, grecv.at[me_g], ms2.at[0], mr2.at[0], dev).start()
+    apart = pl.ds(0, groups - 1)
+    hop2 = batch(grecv.at[apart], grecv.at[apart], ms2.at[0], mr2.at[0])
     grecv[me_g] = gpack[...]
 
     for w in loads[4:11]:
@@ -253,33 +257,30 @@
             preferred_element_type=jnp.float32, precision=lax.Precision.HIGHEST,
         )
     mrecv[me_g] = msend[me_g]
-    metas = []
     for d in range(1, groups):
         g, dev = far(d)
-        metas.append(remote(msend.at[g], mrecv.at[me_g], msem_s.at[d], msem_r.at[d], dev))
-        metas[-1].start()
+        remote(msend.at[g], mrecv.at[me_g], msem_s.at[0], msem_r.at[0], dev).start()
+    metas = batch(msend.at[apart], mrecv.at[apart], msem_s.at[0], msem_r.at[0])
     gt = jnp.where(slot_lane == group * trow + rank_g, 1.0, 0.0)
     gather = gt.T.astype(jnp.bfloat16)
     gt = gt.astype(jnp.bfloat16)
 
-    for m in hop2:
-        m.wait_recv()
+    hop2.wait_recv()
     state = jnp.zeros((part, keys), jnp.float32)
     for g in range(groups - 1):
         step = factor_of(grecv[g, part : part + 16, :])
         state = jnp.where(me_g > g, step * state + grecv[g, 0:part, :].astype(jnp.float32), state)
     for j in range(quad):
         epack[j] = (before_decay[j] * state + before_state[j]).astype(jnp.bfloat16)
-    hop3 = []
     mine_v = pl.ds(pl.multiple_of(me_q * part, part), part)
     for d in range(1, quad):
         j, dev = side(d)
-        hop3.append(remote(epack.at[j], ent.at[mine_v], ms3.at[d], mr3.at[d], dev))
-        hop3[-1].start()
+        remote(epack.at[j], ent.at[mine_v], ms3.at[0], mr3.at[0], dev).start()
     ent[mine_v, :] = epack[me_q]
-    for m in hop3:
-        m.wait_recv()
-    scans = hop1 + hop2 + hop3
+    slices = pl.ds(0, (quad - 1) * part)
+    hop3 = batch(ent.at[slices], ent.at[slices], ms3.at[0], mr3.at[0])
+    hop3.wait_recv()
+    sends = [hop1, hop2, hop3, metas]
     entering = ent[...]
 
     def finish(which):
@@ -333,32 +334,38 @@
         zrecv[pl.ds(groups * trow, pad), :] = jnp.zeros((pad, width), bf)
     far_rows = lambda g: pl.ds(pl.multiple_of(g * trow, 16), trow)
     near_rows = lambda l: pl.ds(pl.multiple_of(l * TILE, TILE), TILE)
-    sends = [mixcopy] + metas + scans
+    sends.append(mixcopy)
     order = arrival_order(me_g, groups)
 
     def home(g):
         return (g * quad + me_q, me_tp)
 
-    def from_far(i):
+    early = [pl.ds(0, 2 * narrow)] + [pl.ds((t + 1) * narrow, narrow) for t in range(1, packs)]
+    late = [pl.ds(t * narrow, narrow) for t in range(packs - 1)]
+    late = late + [pl.ds((packs - 1) * narrow, 2 * narrow)]
+
+    def from_far(i, t):
+        there = (far_rows(order[i]), early[t])
         return remote(
-            sbuf.at[far_rows(order[i])], rbuf.at[far_rows(order[i])],
-            s1.at[i], r1.at[order[i]], home(order[i]),
+            sbuf.at[there], rbuf.at[there], s1.at[0], r1.at[order[i], t], home(order[i])
         )
 
     sbuf[...] = dot(gather, normed[...]).astype(bf)
-    for i, g in enumerate(send_order(me_g, groups)):
-        sends.append(
+    for g in send_order(me_g, groups):
+        for t in range(packs):
             remote(
-                sbuf.at[far_rows(g)], rbuf.at[far_rows(me_g)], s1.at[i], r1.at[me_g], home(g)
-            )
-        )
-        sends[-1].start()
+                sbuf.at[far_rows(g), early[t]], rbuf.at[far_rows(me_g), early[t]],
+                s1.at[0], r1.at[me_g, t], home(g),
+            ).start()
     rbuf[far_rows(me_g), :] = sbuf[far_rows(me_g), :]
-    for m in metas:
-        m.wait_recv()
+    metas.wait_recv()
+    out_rows = pl.ds(0, (groups - 1) * trow)
+    sends.append(batch(sbuf.at[out_rows], sbuf.at[out_rows], s1.at[0], r1.at[0, 0]))
 
     slab = GROUP_SIZE * TILE
     parts = [pl.ds(t * narrow, narrow) for t in range(packs)]
+    taken = [pl.ds((t + 1) * narrow, narrow) for t in range(packs)]
+    lead = pl.ds(0, narrow)
     last = pl.ds(bulk, narrow)
 
     def keys_of(row, t, p):
@@ -384,53 +391,47 @@
     repack = [pairs_of(sq_i, sq_j, t) for t in range(packs)]
     plain_row = lax.broadcasted_iota(jnp.int32, (slab, narrow), 0) % TILE < slots
 
-    def spread(u, src, dst, ss, rr):
-        out = []
+    peers = pl.ds(0, (GROUP_SIZE - 1) * TILE)
+
+    def spread(u, t, src, dst, send, recv):
         for d in range(1, GROUP_SIZE):
             l, dev = near(d)
-            out.append(
-                remote(
-                    src.at[u, near_rows(l)], dst.at[u, near_rows(me_l)],
-                    ss.at[u, d], rr.at[u, d], dev,
-                )
-            )
-            out[-1].start()
-        dst[u, near_rows(me_l), :] = src[u, near_rows(me_l), :]
-        sends.extend(out)
-        return out
+            remote(
+                src.at[u, near_rows(l), parts[t]], dst.at[u, near_rows(me_l), parts[t]],
+                send, recv, dev,
+            ).start()
+        dst[u, near_rows(me_l), parts[t]] = src[u, near_rows(me_l), parts[t]]
 
     def dispatch(u):
-        acc = [jnp.zeros((slab, narrow), jnp.float32) for _ in range(packs)]
-        for p in range(per):
-            i = u * per + p
-            if i > 0:
-                from_far(i).wait_recv()
-            table = mrecv[order[i]][:, 0:trow]
-
-            def pick(t):
-                key = keys_of(down_row, t, p)
-                hit = (key == table[0:1, :]) | (key == table[1:2, :])
-                return jnp.where(hit, 1.0, 0.0).astype(bf)
-
-            plain = pick(None)
-            tail_cols = rbuf[far_rows(order[i]), last]
-            for t in range(packs):
-                acc[t] = acc[t] + dot(plain, rbuf[far_rows(order[i]), parts[t]])
-                acc[t] = acc[t] + dot(pick(t), tail_cols)
+        def pick(p, t):
+            table = mrecv[order[u * per + p]][:, 0:trow]
+            key = keys_of(down_row, t, p)
+            hit = (key == table[0:1, :]) | (key == table[1:2, :])
+            return jnp.where(hit, 1.0, 0.0).astype(bf)
+
+        plain = [pick(p, None) for p in range(per)]
         for t in range(packs):
-            xsend[u, :, parts[t]] = acc[t].astype(bf)
-        return spread(u, xsend, xin, s2, r2)
+            acc = jnp.zeros((slab, narrow), jnp.float32)
+            for p in range(per):
+                i = u * per + p
+                if i > 0:
+                    from_far(i, t).wait_recv()
+                acc = acc + dot(plain[p], rbuf[far_rows(order[i]), taken[t]])
+                acc = acc + dot(pick(p, t), rbuf[far_rows(order[i]), lead])
+            xsend[u, :, parts[t]] = acc.astype(bf)
+            spread(u, t, xsend, xin, s2.at[u], r2.at[u])
+        sends.append(batch(xsend.at[u, peers], xin.at[u, peers], s2.at[u], r2.at[u]))
+        return sends[-1]
 
     def experts(u, arriving):
-        for m in arriving:
-            m.wait_recv()
+        arriving.wait_recv()
         block = xin[u]
         rest = jnp.zeros((slab, narrow), jnp.float32)
         for t in range(packs):
             rest = rest + dot(unpack[t], xin[u, :, parts[t]])
         rest = rest.astype(bf)
-        gated = dot(block, wg[0:bulk, :]) + dot(rest, wg[bulk:width, :])
-        lifted = dot(block, wu[0:bulk, :]) + dot(rest, wu[bulk:width, :])
+        gated = dot(block, wg[narrow:width, :]) + dot(rest, wg[0:narrow, :])
+        lifted = dot(block, wu[narrow:width, :]) + dot(rest, wu[0:narrow, :])
         inner = (silu(gated) * lifted).astype(bf)
         ends = dot(inner, wd[:, last]).astype(bf)
         for t in range(packs):
@@ -438,38 +439,41 @@
             ysend[u, :, parts[t]] = jnp.where(plain_row, main, dot(repack[t], ends)).astype(bf)
 
     def give_back(u):
-        return spread(u, ysend, yrecv, s3, r3)
+        for t in range(packs):
+            spread(u, t, ysend, yrecv, s3.at[u], r3.at[u, t])
+        sends.append(batch(ysend.at[u, peers], ysend.at[u, peers], s3.at[u], r3.at[u, 0]))
+        return [
+            batch(yrecv.at[u, peers, c], yrecv.at[u, peers, c], s3.at[u], r3.at[u, t])
+            for t, c in enumerate(parts)
+        ]
 
     def combine(u, arriving):
-        for m in arriving:
-            m.wait_recv()
-        for p in range(per):
-            i = u * per + p
-            table = mrecv[order[i]].T[0:trow, :]
-
-            def blend(t):
-                key = keys_of(across_row, t, p)
-                both = jnp.where(key == table[:, 0:1], table[:, 2:3], 0.0)
-                both = both + jnp.where(key == table[:, 1:2], table[:, 3:4], 0.0)
-                high = both.astype(bf)
-                return [high, (both - high.astype(jnp.float32)).astype(bf)]
-
-            plain = blend(None)
-            ends = jnp.zeros((trow, narrow), jnp.float32)
-            to = zrecv if i == 0 else zsend
-            for t in range(packs):
-                four = dot(jnp.concatenate(plain + blend(t), axis=0), yrecv[u, :, parts[t]])
-                to[far_rows(order[i]), parts[t]] = (four[0:trow] + four[trow : 2 * trow]).astype(bf)
-                ends = ends + four[2 * trow : 3 * trow] + four[3 * trow : 4 * trow]
-            to[far_rows(order[i]), last] = ends.astype(bf)
-            if i > 0:
-                sends.append(
+        def blend(p, t):
+            table = mrecv[order[u * per + p]].T[0:trow, :]
+            key = keys_of(across_row, t, p)
+            both = jnp.where(key == table[:, 0:1], table[:, 2:3], 0.0)
+            both = both + jnp.where(key == table[:, 1:2], table[:, 3:4], 0.0)
+            high = both.astype(bf)
+            return [high, (both - high.astype(jnp.float32)).astype(bf)]
+
+        plain = [blend(p, None) for p in range(per)]
+        ends = [jnp.zeros((trow, narrow), jnp.float32) for _ in range(per)]
+        for t in range(packs):
+            arriving[t].wait_recv()
+            for p in range(per):
+                i = u * per + p
+                mine_z = far_rows(order[i])
+                to = zrecv if i == 0 else zsend
+                four = dot(jnp.concatenate(plain[p] + blend(p, t), axis=0), yrecv[u, :, parts[t]])
+                to[mine_z, parts[t]] = (four[0:trow] + four[trow : 2 * trow]).astype(bf)
+                ends[p] = ends[p] + four[2 * trow : 3 * trow] + four[3 * trow : 4 * trow]
+                if t == packs - 1:
+                    to[mine_z, last] = ends[p].astype(bf)
+                if i > 0:
                     remote(
-                        zsend.at[far_rows(order[i])], zrecv.at[far_rows(me_g)],
-                        s4.at[i], r4.at[me_g], home(order[i]),
-                    )
-                )
-                sends[-1].start()
+                        zsend.at[mine_z, late[t]], zrecv.at[far_rows(me_g), late[t]],
+                        s4.at[0], r4.at[t], home(order[i]),
+                    ).start()
 
     out0 = dispatch(0)
     weights[1].wait()
@@ -490,13 +494,10 @@
     combine(2, back2)
     combine(3, back3)
     combine(0, back0)
-    for i in range(1, groups):
-        g = order[i]
-        remote(
-            zsend.at[far_rows(g)], zrecv.at[far_rows(g)], s4.at[i], r4.at[g], home(g)
-        ).wait_recv()
-    for c in cols:
+    for t, c in enumerate(late):
+        batch(zsend.at[out_rows, c], zrecv.at[out_rows, c], s4.at[0], r4.at[t]).wait_recv()
         out_ref[:, c] = (merged[:, c].astype(jnp.float32) + dot(gt, zrecv[:, c])).astype(bf)
+    sends.append(batch(zsend.at[out_rows], zsend.at[out_rows], s4.at[0], r4.at[0]))
     for m in sends:
         m.wait_send()
 
@@ -541,7 +542,7 @@
     hb = pl.BlockSpec(memory_space=pl.ANY)
     bf = jnp.bfloat16
     dma = pltpu.SemaphoreType.DMA
-    fd, nd = (groups,), (UNITS, GROUP_SIZE)
+    packs = slab[2] // (width - slab[2])
     inputs = (
         gl, k, v, q, routes.T, group_score[None, :], expert_score.T,
         og, head_gain[None, :], residual, norm_gain[None, :],
@@ -579,9 +580,10 @@
             pltpu.VMEM((groups, part + 16, keys), bf),
             pltpu.VMEM((quad, part, keys), bf),
             pltpu.VMEM((VALUE_DIM, keys), bf),
-            dma((quad,)), dma((quad,)), dma((groups,)), dma((groups,)), dma((quad,)), dma((quad,)),
-            dma((15,)), dma((2,)), dma((groups,)), dma((groups,)),
-            dma(fd), dma(fd), dma(nd), dma(nd), dma(nd), dma(nd), dma(fd), dma(fd),
+            dma((1,)), dma((1,)), dma((1,)), dma((1,)), dma((1,)), dma((1,)),
+            dma((15,)), dma((2,)), dma((1,)), dma((1,)),
+            dma((1,)), dma((groups, packs)), dma((UNITS,)), dma((UNITS,)),
+            dma((UNITS,)), dma((UNITS, packs)), dma((1,)), dma((packs,)),
         ],
         compiler_params=pltpu.CompilerParams(
             collective_id=0, has_side_effects=True, vmem_limit_bytes=60 * 1024 * 1024

time: 67.7 us -> 64.6 us (0.954)
  Pallas kernels: 66.7 us -> 63.7 us
    pallas_call x1, Pallas kernels: 66.7 us -> 63.7 us  [layer_call(): pl.pallas_call(functools.partial(layer_kernel, sp, tp), out_shape=pltpu.V...]
where the time goes in v3:
time: 64.6 us; the launch traced here: 64.5 us
  Pallas kernels  63.7 us (99%)
  local copies, waits for them, and re-layouts  0.8 us (1%)
    pallas_call x1, Pallas kernels, layer_call(): pl.pallas_call(functools.partial(layer_kernel, sp, tp), out_shape=pltpu.V...  63.7 us

profile of v3, /device:TPU:9, one launch (start us, length us, event | category | flops | bytes accessed | tf_op | source)
XLA Modules:
  0.0 64.5 jit_solution(14678271286599236911)
XLA Ops:
  0.0 63.7 %shard_map.145 = bf16[128,2048]{1,0:T(8,128)(2,1)S(1)} custom-call(bf16[256,256]{1,0:T(8,128)(2,1)} %gl_hbm.1, bf16[256,256]{1,0:T(8,128)(2,1)} %k_hbm.1, bf16[256,512]{1,0:T(8,128)(2,1)} %v_hbm.1, bf16[256,256]{1,0:T(8,128)(2,1)} %q_hbm.1, s32[2,128]{1,0:T(2,128)} %bitcast.12, f32[1,128]{1,0:T(1,128)} %bitcast.14, f32[2,128]{1,0:T(2,128)} %bitcast.13, ...), custom_call_target="tpu_custom_call" | custom-call | tf_op jit(solution)/shard_map/pallas_call | solution.py:550
  63.7 0.8 %copy.17 = bf16[128,2048]{1,0:T(8,128)(2,1)} copy(bf16[128,2048]{1,0:T(8,128)(2,1)S(1)} %shard_map.145) | data formatting | bytes 1048576

commit v4 on v3

--- a/solution.py
+++ b/solution.py
@@ -31,7 +31,7 @@
     gl_ref, k_ref, v_ref, q_ref, routes_ref, gscore_ref, escore_ref,
     og_ref, hgain_ref, res_ref, gain_ref, wo, wg, wu, wd, mixin, merged, normed, sbuf, rbuf, xsend, xin, ysend, yrecv, zsend, zrecv,
     msend, mrecv,
-    mix_ref, qlead, within, spack, srecv, gpack, grecv, epack, ent,
+    mix_ref, gather, gated_out, qlead, within, spack, srecv, gpack, grecv, epack, ent,
     ms1, mr1, ms2, mr2, ms3, mr3, isem, mixsem, msem_s, msem_r, s1, r1, s2, r2, s3, r3, s4, r4,
 ):
     rows, width = res_ref.shape
@@ -95,10 +95,12 @@
     pos_i = lax.broadcasted_iota(jnp.int32, (length, length), 0)
     pos_j = lax.broadcasted_iota(jnp.int32, (length, length), 1)
     causal = (pos_i // BLOCK == pos_j // BLOCK) & (pos_j <= pos_i)
-    running = jnp.dot(
-        jnp.where(causal, 1.0, 0.0), logs,
-        preferred_element_type=jnp.float32, precision=lax.Precision.HIGHEST,
-    )
+    ones = jnp.where(causal, 1.0, 0.0).astype(jnp.bfloat16)
+    running = jnp.zeros_like(logs)
+    for _ in range(3):
+        piece = logs.astype(jnp.bfloat16)
+        running = running + dot(ones, piece)
+        logs = logs - piece.astype(jnp.float32)
     split = [slice(n * BLOCK, (n + 1) * BLOCK) for n in range(blocks)]
     closing = [running[(n + 1) * BLOCK - 1 : (n + 1) * BLOCK, :] for n in range(blocks)]
     loads[1].wait()
@@ -262,8 +264,11 @@
         remote(msend.at[g], mrecv.at[me_g], msem_s.at[0], msem_r.at[0], dev).start()
     metas = batch(msend.at[apart], mrecv.at[apart], msem_s.at[0], msem_r.at[0])
     gt = jnp.where(slot_lane == group * trow + rank_g, 1.0, 0.0)
-    gather = gt.T.astype(jnp.bfloat16)
+    gather[...] = gt.T.astype(jnp.bfloat16)
     gt = gt.astype(jnp.bfloat16)
+    for h in range(heads):
+        hv = slice(h * VALUE_DIM, (h + 1) * VALUE_DIM)
+        gated_out[:, hv] = hgain_ref[...] * silu(og_ref[:, hv].astype(jnp.float32))
 
     hop2.wait_recv()
     state = jnp.zeros((part, keys), jnp.float32)
@@ -293,10 +298,8 @@
                 preferred_element_type=jnp.float32,
             )
             mean = jnp.mean(attended * attended, axis=1, keepdims=True)
-            unit = attended * lax.rsqrt(mean + 1e-06) * hgain_ref[...]
-            mix_ref[at, hv] = (unit * silu(og_ref[at, hv].astype(jnp.float32))).astype(
-                jnp.bfloat16
-            )
+            unit = attended * lax.rsqrt(mean + 1e-06)
+            mix_ref[at, hv] = (unit * gated_out[at, hv]).astype(jnp.bfloat16)
 
     other = 1 - me_tp
     finish(other)
@@ -350,14 +353,15 @@
             sbuf.at[there], rbuf.at[there], s1.at[0], r1.at[order[i], t], home(order[i])
         )
 
-    sbuf[...] = dot(gather, normed[...]).astype(bf)
+    ready = normed[...]
     for g in send_order(me_g, groups):
+        sbuf[far_rows(g), :] = dot(gather[far_rows(g), :], ready).astype(bf)
         for t in range(packs):
             remote(
                 sbuf.at[far_rows(g), early[t]], rbuf.at[far_rows(me_g), early[t]],
                 s1.at[0], r1.at[me_g, t], home(g),
             ).start()
-    rbuf[far_rows(me_g), :] = sbuf[far_rows(me_g), :]
+    rbuf[far_rows(me_g), :] = dot(gather[far_rows(me_g), :], ready).astype(bf)
     metas.wait_recv()
     out_rows = pl.ds(0, (groups - 1) * trow)
     sends.append(batch(sbuf.at[out_rows], sbuf.at[out_rows], s1.at[0], r1.at[0, 0]))
@@ -479,18 +483,18 @@
     weights[1].wait()
     weights[2].wait()
     weights[3].wait()
+    out1 = dispatch(1)
     experts(0, out0)
-    out1 = dispatch(1)
     out2 = dispatch(2)
     experts(1, out1)
+    back1 = give_back(1)
     out3 = dispatch(3)
-    back1 = give_back(1)
     experts(2, out2)
     back2 = give_back(2)
+    combine(1, back1)
     experts(3, out3)
     back3 = give_back(3)
     back0 = give_back(0)
-    combine(1, back1)
     combine(2, back2)
     combine(3, back3)
     combine(0, back0)
@@ -572,6 +576,8 @@
             pltpu.VMEM((groups, 8, 128), jnp.float32),
             pltpu.VMEM((groups, 8, 128), jnp.float32),
             pltpu.VMEM(v.shape, bf),
+            pltpu.VMEM((lanes, rows), bf),
+            pltpu.VMEM(v.shape, jnp.float32),
             pltpu.VMEM(q.shape, bf),
             pltpu.VMEM(v.shape, jnp.float32),
             pltpu.VMEM((quad, part + 16, keys), bf),

time: 64.6 us -> 60.8 us (0.941)
  Pallas kernels: 63.7 us -> 59.8 us
    pallas_call x1, Pallas kernels: 63.7 us -> 59.8 us  [layer_call(): pl.pallas_call(functools.partial(layer_kernel, sp, tp), out_shape=pltpu.V...]
where the time goes in v4:
time: 60.8 us; the launch traced here: 60.6 us
  Pallas kernels  59.8 us (98%)
  local copies, waits for them, and re-layouts  0.8 us (1%)
    pallas_call x1, Pallas kernels, layer_call(): pl.pallas_call(functools.partial(layer_kernel, sp, tp), out_shape=pltpu.V...  59.8 us

profile of v4, /device:TPU:9, one launch (start us, length us, event | category | flops | bytes accessed | tf_op | source)
XLA Modules:
  0.0 60.6 jit_solution(839366741534710878)
XLA Ops:
  0.0 59.8 %shard_map.145 = bf16[128,2048]{1,0:T(8,128)(2,1)S(1)} custom-call(bf16[256,256]{1,0:T(8,128)(2,1)} %gl_hbm.1, bf16[256,256]{1,0:T(8,128)(2,1)} %k_hbm.1, bf16[256,512]{1,0:T(8,128)(2,1)} %v_hbm.1, bf16[256,256]{1,0:T(8,128)(2,1)} %q_hbm.1, s32[2,128]{1,0:T(2,128)} %bitcast.12, f32[1,128]{1,0:T(1,128)} %bitcast.14, f32[2,128]{1,0:T(2,128)} %bitcast.13, ...), custom_call_target="tpu_custom_call" | custom-call | tf_op jit(solution)/shard_map/pallas_call | solution.py:554
  59.8 0.8 %copy.17 = bf16[128,2048]{1,0:T(8,128)(2,1)} copy(bf16[128,2048]{1,0:T(8,128)(2,1)S(1)} %shard_map.145) | data formatting | bytes 1048576

commit v5 on v4

--- a/solution.py
+++ b/solution.py
@@ -424,6 +424,8 @@
                 acc = acc + dot(pick(p, t), rbuf[far_rows(order[i]), lead])
             xsend[u, :, parts[t]] = acc.astype(bf)
             spread(u, t, xsend, xin, s2.at[u], r2.at[u])
+
+    def dispatched(u):
         sends.append(batch(xsend.at[u, peers], xin.at[u, peers], s2.at[u], r2.at[u]))
         return sends[-1]
 
@@ -445,6 +447,8 @@
     def give_back(u):
         for t in range(packs):
             spread(u, t, ysend, yrecv, s3.at[u], r3.at[u, t])
+
+    def given_back(u):
         sends.append(batch(ysend.at[u, peers], ysend.at[u, peers], s3.at[u], r3.at[u, 0]))
         return [
             batch(yrecv.at[u, peers, c], yrecv.at[u, peers, c], s3.at[u], r3.at[u, t])
@@ -479,25 +483,39 @@
                         s4.at[0], r4.at[t], home(order[i]),
                     ).start()
 
-    out0 = dispatch(0)
+    inner = me_g % 2 + me_g // 2 - 2 * (me_g % 2) * (me_g // 2)
+
+    def at_edge(step, u):
+        if groups != 4:
+            step(u)
+        else:
+            pl.when(inner == 0)(lambda: step(u))
+
+    def at_inner(step, u):
+        if groups == 4:
+            pl.when(inner == 1)(lambda: step(u))
+
+    dispatch(0)
+    dispatch(1)
     weights[1].wait()
     weights[2].wait()
     weights[3].wait()
-    out1 = dispatch(1)
-    experts(0, out0)
-    out2 = dispatch(2)
-    experts(1, out1)
-    back1 = give_back(1)
-    out3 = dispatch(3)
-    experts(2, out2)
-    back2 = give_back(2)
-    combine(1, back1)
-    experts(3, out3)
-    back3 = give_back(3)
-    back0 = give_back(0)
-    combine(2, back2)
-    combine(3, back3)
-    combine(0, back0)
+    experts(0, dispatched(0))
+    at_inner(give_back, 0)
+    at_edge(dispatch, 2)
+    experts(1, dispatched(1))
+    give_back(1)
+    at_inner(dispatch, 2)
+    dispatch(3)
+    experts(2, dispatched(2))
+    give_back(2)
+    combine(1, given_back(1))
+    experts(3, dispatched(3))
+    give_back(3)
+    at_edge(give_back, 0)
+    combine(2, given_back(2))
+    combine(3, given_back(3))
+    combine(0, given_back(0))
     for t, c in enumerate(late):
         batch(zsend.at[out_rows, c], zrecv.at[out_rows, c], s4.at[0], r4.at[t]).wait_recv()
         out_ref[:, c] = (merged[:, c].astype(jnp.float32) + dot(gt, zrecv[:, c])).astype(bf)
@@ -515,13 +533,13 @@
 def send_order(me, count):
     if count != 4:
         return [lax.rem(me + d, count) for d in range(1, count)]
-    return by_place(me, ((3, 1, 2), (3, 2, 0), (0, 1, 3), (0, 2, 1)))
+    return by_place(me, ((1, 3, 2), (3, 2, 0), (0, 1, 3), (2, 0, 1)))
 
 
 def arrival_order(me, count):
     if count != 4:
         return [me] + [lax.rem(me + count - d, count) for d in range(1, count)]
-    return [me] + by_place(me, ((3, 2, 1), (0, 3, 2), (3, 0, 1), (0, 1, 2)))
+    return [me] + by_place(me, ((2, 3, 1), (0, 3, 2), (3, 0, 1), (1, 0, 2)))
 
 
 def rbuf_rows(rows, sp, tp):

time: 60.8 us -> 60.8 us (level)
  no operation moved by 1% of the time
where the time goes in v5:
time: 60.8 us; the launch traced here: 60.6 us
  Pallas kernels  59.8 us (98%)
  local copies, waits for them, and re-layouts  0.8 us (1%)
    pallas_call x1, Pallas kernels, layer_call(): pl.pallas_call(functools.partial(layer_kernel, sp, tp), out_shape=pltpu.V...  59.8 us

profile of v5, /device:TPU:9, one launch (start us, length us, event | category | flops | bytes accessed | tf_op | source)
XLA Modules:
  0.0 60.6 jit_solution(10096228484824561225)
XLA Ops:
  0.0 59.8 %shard_map.145 = bf16[128,2048]{1,0:T(8,128)(2,1)S(1)} custom-call(bf16[256,256]{1,0:T(8,128)(2,1)} %gl_hbm.1, bf16[256,256]{1,0:T(8,128)(2,1)} %k_hbm.1, bf16[256,512]{1,0:T(8,128)(2,1)} %v_hbm.1, bf16[256,256]{1,0:T(8,128)(2,1)} %q_hbm.1, s32[2,128]{1,0:T(2,128)} %bitcast.12, f32[1,128]{1,0:T(1,128)} %bitcast.14, f32[2,128]{1,0:T(2,128)} %bitcast.13, ...), custom_call_target="tpu_custom_call" | custom-call | tf_op jit(solution)/shard_map/pallas_call | solution.py:572
  59.8 0.8 %copy.17 = bf16[128,2048]{1,0:T(8,128)(2,1)} copy(bf16[128,2048]{1,0:T(8,128)(2,1)S(1)} %shard_map.145) | data formatting | bytes 1048576
